TPU v7x, 32 devices: a whole 2x2x4 slice. The times are simulated.
32 devices in a mesh: rep: 2 (over x), fs: 8 (over z, y), tp: 2 (over core).
Axes of the slice: x: 2, y: 2, z: 4, core: 2. Of those that a mesh axis runs over, the one named last changes fastest.
Arguments:
- tokens: bfloat16 [4096, 1024], P(('rep', 'fs', 'tp')), may hold values from -4 to 4
- mixer_out: bfloat16 [4096, 1024], P(('rep', 'fs')), may hold values from -4 to 4
- gain_first: float32 [1024], replicated, may hold values from 0.1 to 1.9
- gate_first: bfloat16 [1024, 2816], P('fs', 'tp'), may hold values from -0.1875 to 0.1875
- up_first: bfloat16 [1024, 2816], P('fs', 'tp'), may hold values from -0.1875 to 0.1875
- down_first: bfloat16 [2816, 1024], P('tp', 'fs'), may hold values from -0.109375 to 0.109375
- gain_second: float32 [1024], replicated, may hold values from 0.1 to 1.9
- gate_second: bfloat16 [1024, 2816], P('fs', 'tp'), may hold values from -0.1875 to 0.1875
- up_second: bfloat16 [1024, 2816], P('fs', 'tp'), may hold values from -0.1875 to 0.1875
- down_second: bfloat16 [2816, 1024], P('tp', 'fs'), may hold values from -0.109375 to 0.109375
- gain_last: float32 [1024], P('tp'), may hold values from 0.1 to 1.9
Outputs:
- result: bfloat16 [4096, 1024], P(('rep', 'fs'), 'tp')
All inputs are finite; a program needn't handle non-finite values.
Results may differ from a plain program's by a relative error of at most 0.02.
Values may be sent and summed in bfloat16 or wider, within the bound.
A program may use at most 64 MiB of HBM per device.

v0:
```python
import jax
import jax.numpy as jnp
from jax import lax
from jax.sharding import PartitionSpec as P

EPS = 1e-06


def over_all(slab, axis, dim):

    def gathered(part):
        return lax.all_gather(part, axis, axis=dim, tiled=True)

    return jax.tree.map(gathered, slab)


def normalize(floats_in, gain_vec):
    floats = floats_in.astype(jnp.float32)
    factor = lax.rsqrt(jnp.mean(floats * floats, axis=-1, keepdims=True) + EPS)
    return (floats * factor * gain_vec.astype(jnp.float32)).astype(jnp.bfloat16)


def gather_group(row_block):
    return lax.all_gather(row_block, "tp", axis=0, tiled=True)


def inner_hidden(normed, w_gate, w_up):

    def add_both(totals, pieces):
        columns = lax.slice_in_dim(normed, 0, pieces[0].shape[0], axis=1)
        return (
            totals[0] + jnp.dot(columns, pieces[0], preferred_element_type=jnp.float32),
            totals[1] + jnp.dot(columns, pieces[1], preferred_element_type=jnp.float32),
        )

    empty = jnp.zeros((normed.shape[0], w_gate.shape[1]), jnp.float32)
    gate_acc, up_acc = add_both((empty, empty), over_all((w_gate, w_up), "fs", 0))
    return (jax.nn.silu(gate_acc) * up_acc).astype(jnp.bfloat16)


def outer_weight(w_down):
    return lax.all_gather(w_down, "fs", axis=1, tiled=True)


def local(
    tokens,
    mixer_out,
    gain_first,
    gate_first,
    up_first,
    down_first,
    gain_second,
    gate_second,
    up_second,
    down_second,
    gain_last,
):
    rows_dev = tokens.shape[0]
    tp_count = lax.axis_size("tp")
    tp_index = lax.axis_index("tp")
    normed_own = normalize(tokens, gain_first)
    normed_one = gather_group(normed_own)
    hidden_one = inner_hidden(normed_one, gate_first, up_first)
    down_full = outer_weight(down_first)

    def row_terms():
        picked = lax.slice_in_dim(hidden_one, 0, rows_dev * lax.axis_size("tp"), axis=0)
        return jnp.dot(picked, down_full, preferred_element_type=jnp.float32)

    ffn_one = lax.psum_scatter(
        row_terms().astype(jnp.bfloat16), "tp", scatter_dimension=0, tiled=True
    ).astype(jnp.float32)
    after_one = (tokens.astype(jnp.float32) + 0.5 * ffn_one).astype(jnp.bfloat16)
    own_mixer = lax.dynamic_slice_in_dim(mixer_out, tp_index * rows_dev, rows_dev, 0)
    mixed_in = (after_one.astype(jnp.float32) + own_mixer.astype(jnp.float32)).astype(jnp.bfloat16)
    gathered = gather_group(mixed_in)
    normed_two = normalize(gathered, gain_second)
    hidden_two = inner_hidden(normed_two, gate_second, up_second)
    down_two_full = outer_weight(down_second)
    terms_two = jnp.dot(hidden_two, down_two_full, preferred_element_type=jnp.float32)
    ffn_two = lax.psum_scatter(
        terms_two.astype(jnp.bfloat16), "tp", scatter_dimension=1, tiled=True
    ).astype(jnp.float32)
    col_width = ffn_two.shape[1]
    my_cols = lax.dynamic_slice_in_dim(gathered, tp_index * col_width, col_width, 1)
    after_two = (my_cols.astype(jnp.float32) + 0.5 * ffn_two).astype(jnp.bfloat16)
    floats = after_two.astype(jnp.float32)
    sum_sq = lax.psum(jnp.sum(floats * floats, axis=1), "tp")
    factor = lax.rsqrt(sum_sq / (col_width * tp_count) + EPS)
    return (floats * factor[:, None] * gain_last.astype(jnp.float32)[None, :]).astype(jnp.bfloat16)


def solution(mesh):
    in_specs = (
        P(("rep", "fs", "tp"), None),
        P(("rep", "fs"), None),
        P(),
        P("fs", "tp"),
        P("fs", "tp"),
        P("tp", "fs"),
        P(),
        P("fs", "tp"),
        P("fs", "tp"),
        P("tp", "fs"),
        P("tp"),
    )
    out_specs = P(("rep", "fs"), "tp")
    return jax.shard_map(local, mesh=mesh, in_specs=in_specs, out_specs=out_specs, check_vma=False)
```

profile of v0, /device:TPU:0, one launch (start us, length us, event | category | flops | bytes accessed | tf_op | source)
XLA Modules:
  0.0 402.3 jit_solution(16282262251810732455)
XLA Ops:
  6.5 0.7 all-gather.7.cloned.1.call-update
  7.3 0.7 all-gather.11.cloned.1.call-update
  8.1 0.7 all-gather.9.cloned.1.call-update
  8.8 1.1 fusion.10
  9.9 1.1 fusion.12
  11.0 2.3 all_gather.24
  13.3 56.3 %all-gather.7.cloned.1.call-done = bf16[1024,1408]{1,0:T(8,128)(2,1)} async-done(((bf16[128,1408]{1,0:T(8,128)(2,1)}), bf16[1024,1408]{1,0:T(8,128)(2,1)}) %all-gather.7.cloned.1.call-update) | async-done | bytes 2883600 | tf_op jit(solution)/shard_map/all_gather | solution.py:12
  69.6 2.8 fusion.20
  72.4 57.4 %all-gather.11.cloned.1.call-done = bf16[1408,1024]{1,0:T(8,128)(2,1)} async-done(((bf16[1408,128]{1,0:T(8,128)(2,1)}), bf16[1408,1024]{1,0:T(8,128)(2,1)}) %all-gather.11.cloned.1.call-update) | async-done | bytes 2883600 | tf_op jit(solution)/shard_map/all_gather | solution.py:42
  129.8 57.7 %all-gather.9.cloned.1.call-done = bf16[1024,1408]{1,0:T(8,128)(2,1)} async-done(((bf16[128,1408]{1,0:T(8,128)(2,1)}), bf16[1024,1408]{1,0:T(8,128)(2,1)}) %all-gather.9.cloned.1.call-update) | async-done | bytes 2883600 | tf_op jit(solution)/shard_map/all_gather | solution.py:12
  187.5 5.4 %convolution_convert_fusion.1 = bf16[256,1024]{1,0:T(8,128)(2,1)} fusion(bf16[1408,1024]{1,0:T(8,128)(2,1)} %all-gather.11.cloned.1.call-done, bf16[256,1024]{1,0:T(8,128)(2,1)S(1)} %all_gather.24, bf16[1024,1408]{1,0:T(8,128)(2,1)} %all-gather.9.cloned.1.call-done, f32[256,1408]{1,0:T(8,128)S(1)} %fusion.20), kind=kOutput, calls=%fused_computation.7 | convolution fusion | flops 1478819840 | bytes 8257536 | tf_op jit(solution)/shard_map/dot_general | solution.py:68
  194.2 0.7 all-gather.17.cloned.1.call-update
  194.9 4.7 %reduce-scatter.3.cloned.1.call-done = bf16[128,1024]{1,0:T(8,128)(2,1)} async-done(((bf16[256,1024]{1,0:T(8,128)(2,1)}), bf16[128,1024]{1,0:T(8,128)(2,1)}) %reduce-scatter.3.cloned.1.call-update) | async-done | bytes 262160 | tf_op jit(solution)/shard_map/reduce_scatter | solution.py:70
  199.7 1.1 add_convert_fusion.1
  200.7 2.2 all_gather.28
  203.1 57.0 %all-gather.13.cloned.1.call-done = bf16[1024,1408]{1,0:T(8,128)(2,1)} async-done(((bf16[128,1408]{1,0:T(8,128)(2,1)}), bf16[1024,1408]{1,0:T(8,128)(2,1)}) %all-gather.13.cloned.1.call-update) | async-done | bytes 2883600 | tf_op jit(solution)/shard_map/all_gather | solution.py:12
  260.2 2.9 fusion.16
  263.0 55.1 %all-gather.15.cloned.1.call-done = bf16[1024,1408]{1,0:T(8,128)(2,1)} async-done(((bf16[128,1408]{1,0:T(8,128)(2,1)}), bf16[1024,1408]{1,0:T(8,128)(2,1)}) %all-gather.15.cloned.1.call-update) | async-done | bytes 2883600 | tf_op jit(solution)/shard_map/all_gather | solution.py:12
  318.1 60.3 %all-gather.17.cloned.1.call-done = bf16[1408,1024]{1,0:T(8,128)(2,1)} async-done(((bf16[1408,128]{1,0:T(8,128)(2,1)}), bf16[1408,1024]{1,0:T(8,128)(2,1)}) %all-gather.17.cloned.1.call-update) | async-done | bytes 2883600 | tf_op jit(solution)/shard_map/all_gather | solution.py:42
  378.4 5.4 %convolution_convert_fusion = bf16[256,1024]{1,0:T(8,128)(2,1)} fusion(bf16[1408,1024]{1,0:T(8,128)(2,1)} %all-gather.17.cloned.1.call-done, bf16[1024,1408]{1,0:T(8,128)(2,1)} %all-gather.15.cloned.1.call-done, f32[256,1408]{1,0:T(8,128)S(1)} %fusion.16, bf16[256,1024]{1,0:T(8,128)(2,1)S(1)} %all_gather.28, f32[1024]{0:T(1024)S(1)} %copy-done.2, ...), kind=kOutput, calls=%fused_computation.6 | convolution fusion | flops 1479868416 | bytes 8262656 | tf_op jit(solution)/shard_map/dot_general | solution.py:80
  383.8 6.3 %reduce-scatter.5.cloned.1.call-done = bf16[256,512]{1,0:T(8,128)(2,1)} async-done(((bf16[256,1024]{1,0:T(8,128)(2,1)}), bf16[256,512]{1,0:T(8,128)(2,1)}) %reduce-scatter.5.cloned.1.call-update) | async-done | bytes 262160 | tf_op jit(solution)/shard_map/reduce_scatter | solution.py:81
  390.1 1.1 fusion.7
  391.2 2.5 psum.7
  393.7 1.8 fusion.9
  (24 shorter events, 1.6 us)
Async XLA Ops:
  6.5 63.0 %all-gather.7.cloned.1.call-start = ((), (), s32[]{:S(2)}) async-start(), calls=%async_computation.2 | async-start | bytes 3244032 | tf_op jit(solution)/shard_map/all_gather | solution.py:12
  7.3 122.6 %all-gather.11.cloned.1.call-start = ((), (), s32[]{:S(2)}) async-start(), calls=%async_computation.4 | async-start | bytes 3244032 | tf_op jit(solution)/shard_map/all_gather | solution.py:42
  8.0 179.5 %all-gather.9.cloned.1.call-start = ((), (), s32[]{:S(2)}) async-start(), calls=%async_computation.3 | async-start | bytes 3244032 | tf_op jit(solution)/shard_map/all_gather | solution.py:12
  8.7 190.9 %reduce-scatter.3.cloned.1.call-start = ((), (), s32[]{:S(2)}) async-start(), calls=%async_computation.5 | async-start | bytes 786432 | tf_op jit(solution)/shard_map/reduce_scatter | solution.py:70
  72.4 127.3 %copy-start = (bf16[128,1024]{1,0:T(8,128)(2,1)S(1)}, bf16[128,1024]{1,0:T(8,128)(2,1)}, u32[]{:S(2)}) copy-start(bf16[128,1024]{1,0:T(8,128)(2,1)} %param.11) | copy-start | bytes 786436
  72.4 127.3 %copy-start.1 = (bf16[256,1024]{1,0:T(8,128)(2,1)S(1)}, bf16[256,1024]{1,0:T(8,128)(2,1)}, u32[]{:S(2)}) copy-start(bf16[256,1024]{1,0:T(8,128)(2,1)} %param.12) | copy-start | bytes 1572868
  192.9 67.2 %copy-start.2 = (f32[1024]{0:T(1024)S(1)}, f32[1024]{0:T(1024)}, u32[]{:S(2)}) copy-start(f32[1024]{0:T(1024)} %param.17) | copy-start | bytes 12292
  193.0 67.2 %all-gather.13.cloned.1.call-start = ((), (), s32[]{:S(2)}) async-start(), calls=%async_computation.6 | async-start | bytes 3244032 | tf_op jit(solution)/shard_map/all_gather | solution.py:12
  193.5 124.6 %all-gather.15.cloned.1.call-start = ((), (), s32[]{:S(2)}) async-start(), calls=%async_computation.7 | async-start | bytes 3244032 | tf_op jit(solution)/shard_map/all_gather | solution.py:12
  194.1 184.3 %all-gather.17.cloned.1.call-start = ((), (), s32[]{:S(2)}) async-start(), calls=%async_computation.8 | async-start | bytes 3244032 | tf_op jit(solution)/shard_map/all_gather | solution.py:42
  194.9 195.2 %reduce-scatter.5.cloned.1.call-start = ((), (), s32[]{:S(2)}) async-start(), calls=%async_computation.9 | async-start | bytes 786432 | tf_op jit(solution)/shard_map/reduce_scatter | solution.py:81
  263.0 130.7 %copy-start.3 = (f32[512]{0:T(512)S(1)}, f32[512]{0:T(512)}, u32[]{:S(2)}) copy-start(f32[512]{0:T(512)} %param.21) | copy-start | bytes 6148
Sparse Core Ops, SparseCore 0:
  9.5 60.0 all-gather.6
  71.6 58.1 all-gather.10
  132.0 55.4 all-gather.8
  193.1 6.5 reduce-scatter.2
  201.7 58.4 all-gather.12
  262.2 55.9 all-gather.14
  320.2 58.1 all-gather.16
  384.0 6.0 reduce-scatter.4
where the time goes:
time: 403 us; the launch traced here: 402 us
  waiting for transfers between devices  359 us (89%)
  matrix products  16.5 us (4%)
  between operations  13.6 us (3%)
  blocking collectives  6.95 us (2%)
  other arithmetic  6.36 us (2%)
    all_gather x4, waiting for transfers between devices, gathered(): return lax.all_gather(part, axis, axis=dim, tiled=True)  226 us
    all_gather x2, waiting for transfers between devices, outer_weight(): return lax.all_gather(w_down, 'fs', axis=1, tiled=True)  118 us
  transfers between devices with their start and end apart: 8, of which 8 were waited for; matrix products, arithmetic and copies ran while one was open for 2% of the time, Pallas kernels for 0%

commit v1 on v0

--- a/solution.py
+++ b/solution.py
@@ -4,6 +4,12 @@
 from jax.sharding import PartitionSpec as P
 
 EPS = 1e-06
+
+
+def all_parts(x, mesh_axis, along):
+    pieces = lax.all_gather(x, mesh_axis, axis=0, tiled=False)
+    whole = jnp.concatenate(pieces, axis=along)
+    return whole
 
 
 def over_all(slab, axis, dim):
@@ -39,7 +45,7 @@
 
 
 def outer_weight(w_down):
-    return lax.all_gather(w_down, "fs", axis=1, tiled=True)
+    return all_parts(w_down, "fs", 1)
 
 
 def local(

time: 403 us -> 396 us (0.983)
  waiting for transfers between devices: 359 us -> 343 us
  local copies, waits for them, and re-layouts: 0.02 us -> 6.67 us
    all_gather x2, waiting for transfers between devices: 118 us -> 107 us  [all_parts(): pieces = lax.all_gather(x, mesh_axis, axis=0, tiled=False)]
    reshape x0 -> x2, local copies, waits for them, and re-layouts: none -> 6.66 us  [all_parts(): whole = jnp.concatenate(pieces, axis=along)]
    all_gather x4, waiting for transfers between devices: 226 us -> 220 us  [gathered(): return lax.all_gather(part, axis, axis=dim, tiled=True)]
  transfers between devices with their start and end apart: 8 -> 8, of which waited for: 8 -> 8; matrix products, arithmetic and copies ran while one was open for 2% -> 6% of each run, Pallas kernels for 0% -> 0%
where the time goes in v1:
time: 396 us; the launch traced here: 395 us
  waiting for transfers between devices  343 us (87%)
  matrix products  17.8 us (4%)
  between operations  13.5 us (3%)
  blocking collectives  6.95 us (2%)
  local copies, waits for them, and re-layouts  6.67 us (2%)
  other arithmetic  6.44 us (2%)
    all_gather x4, waiting for transfers between devices, gathered(): return lax.all_gather(part, axis, axis=dim, tiled=True)  220 us
    all_gather x2, waiting for transfers between devices, all_parts(): pieces = lax.all_gather(x, mesh_axis, axis=0, tiled=False)  107 us
    dot_general x2, matrix products, add_both(): jnp.dot(columns, pieces[0], preferred_element_type=jnp.float32)  7.96 us
  transfers between devices with their start and end apart: 8, of which 8 were waited for; matrix products, arithmetic and copies ran while one was open for 6% of the time, Pallas kernels for 0%

profile of v1, /device:TPU:0, one launch (start us, length us, event | category | flops | bytes accessed | tf_op | source)
XLA Modules:
  0.0 395.1 jit_solution(15235929821668697075)
XLA Ops:
  6.5 0.7 all-gather.17.cloned.1.call-update
  7.3 0.7 all-gather.9.cloned.1.call-update
  9.4 1.1 fusion.10
  10.5 1.1 fusion.12
  11.6 2.3 all_gather.30
  13.9 55.7 %all-gather.17.cloned.1.call-done = bf16[11264,128]{1,0:T(8,128)(2,1)} async-done(((bf16[1408,128]{1,0:T(8,128)(2,1)}), bf16[11264,128]{1,0:T(8,128)(2,1)}) %all-gather.17.cloned.1.call-update) | async-done | bytes 2883600 | tf_op jit(solution)/shard_map/all_gather | solution.py:10
  69.6 3.3 copy.12
  72.9 54.8 %all-gather.9.cloned.1.call-done = bf16[1024,1408]{1,0:T(8,128)(2,1)} async-done(((bf16[128,1408]{1,0:T(8,128)(2,1)}), bf16[1024,1408]{1,0:T(8,128)(2,1)}) %all-gather.9.cloned.1.call-update) | async-done | bytes 2883600 | tf_op jit(solution)/shard_map/all_gather | solution.py:18
  127.7 4.0 %fusion.20 = f32[256,1408]{1,0:T(8,128)} fusion(bf16[256,1024]{1,0:T(8,128)(2,1)S(1)} %all_gather.30, bf16[1024,1408]{1,0:T(8,128)(2,1)} %all-gather.9.cloned.1.call-done), kind=kOutput, calls=%fused_computation.33 | convolution fusion | flops 738197504 | bytes 4849664 | tf_op jit(solution)/shard_map/dot_general | solution.py:38
  131.7 54.2 %all-gather.11.cloned.1.call-done = bf16[1024,1408]{1,0:T(8,128)(2,1)} async-done(((bf16[128,1408]{1,0:T(8,128)(2,1)}), bf16[1024,1408]{1,0:T(8,128)(2,1)}) %all-gather.11.cloned.1.call-update) | async-done | bytes 2883600 | tf_op jit(solution)/shard_map/all_gather | solution.py:18
  185.9 4.9 %convolution_convert_fusion.1 = bf16[256,1024]{1,0:T(8,128)(2,1)} fusion(bf16[1408,1024]{0,1:T(8,128)(2,1)S(1)} %bitcast.19, bf16[256,1024]{1,0:T(8,128)(2,1)S(1)} %all_gather.30, bf16[1024,1408]{1,0:T(8,128)(2,1)} %all-gather.11.cloned.1.call-done, f32[256,1408]{1,0:T(8,128)} %fusion.20), kind=kOutput, calls=%fused_computation.7 | convolution fusion | flops 1478819840 | bytes 8257536 | tf_op jit(solution)/shard_map/dot_general | solution.py:74
  192.1 51.7 %all-gather.19.cloned.1.call-done = bf16[11264,128]{1,0:T(8,128)(2,1)} async-done(((bf16[1408,128]{1,0:T(8,128)(2,1)}), bf16[11264,128]{1,0:T(8,128)(2,1)}) %all-gather.19.cloned.1.call-update) | async-done | bytes 2883600 | tf_op jit(solution)/shard_map/all_gather | solution.py:10
  243.9 3.3 copy.13
  247.2 5.3 %reduce-scatter.3.cloned.1.call-done = bf16[128,1024]{1,0:T(8,128)(2,1)} async-done(((bf16[256,1024]{1,0:T(8,128)(2,1)}), bf16[128,1024]{1,0:T(8,128)(2,1)}) %reduce-scatter.3.cloned.1.call-update) | async-done | bytes 262160 | tf_op jit(solution)/shard_map/reduce_scatter | solution.py:76
  252.5 1.2 add_convert_fusion.1
  253.7 2.2 all_gather.35
  256.1 57.0 %all-gather.13.cloned.1.call-done = bf16[1024,1408]{1,0:T(8,128)(2,1)} async-done(((bf16[128,1408]{1,0:T(8,128)(2,1)}), bf16[1024,1408]{1,0:T(8,128)(2,1)}) %all-gather.13.cloned.1.call-update) | async-done | bytes 2883600 | tf_op jit(solution)/shard_map/all_gather | solution.py:18
  313.0 4.0 %fusion.16 = f32[256,1408]{1,0:T(8,128)} fusion(bf16[1024,1408]{1,0:T(8,128)(2,1)} %all-gather.13.cloned.1.call-done, bf16[256,1024]{1,0:T(8,128)(2,1)S(1)} %all_gather.35, f32[1024]{0:T(1024)S(1)} %copy-done.1, f32[256]{0:T(256)S(1)} %add_rsqrt_fusion.1), kind=kOutput, calls=%fused_computation.27 | convolution fusion | flops 739246080 | bytes 4854784 | tf_op jit(solution)/shard_map/dot_general | solution.py:38
  317.0 54.1 %all-gather.15.cloned.1.call-done = bf16[1024,1408]{1,0:T(8,128)(2,1)} async-done(((bf16[128,1408]{1,0:T(8,128)(2,1)}), bf16[1024,1408]{1,0:T(8,128)(2,1)}) %all-gather.15.cloned.1.call-update) | async-done | bytes 2883600 | tf_op jit(solution)/shard_map/all_gather | solution.py:18
  371.2 4.9 %convolution_convert_fusion = bf16[256,1024]{1,0:T(8,128)(2,1)} fusion(bf16[1408,1024]{0,1:T(8,128)(2,1)S(1)} %bitcast.18, bf16[1024,1408]{1,0:T(8,128)(2,1)} %all-gather.15.cloned.1.call-done, f32[256,1408]{1,0:T(8,128)} %fusion.16, bf16[256,1024]{1,0:T(8,128)(2,1)S(1)} %all_gather.35, f32[1024]{0:T(1024)S(1)} %copy-done.1, f32[256]{0:T(256)S(1)} %add_rsqrt_fusion.1), kind=kOutput, calls=%fused_computation.6 | convolution fusion | flops 1479868416 | bytes 8262656 | tf_op jit(solution)/shard_map/dot_general | solution.py:86
  376.1 6.7 %reduce-scatter.5.cloned.1.call-done = bf16[256,512]{1,0:T(8,128)(2,1)} async-done(((bf16[256,1024]{1,0:T(8,128)(2,1)}), bf16[256,512]{1,0:T(8,128)(2,1)}) %reduce-scatter.5.cloned.1.call-update) | async-done | bytes 262160 | tf_op jit(solution)/shard_map/reduce_scatter | solution.py:87
  382.8 1.1 fusion.7
  384.0 2.5 psum.7
  386.4 1.8 fusion.9
  (24 shorter events, 2.9 us)
Async XLA Ops:
  6.5 63.0 %all-gather.17.cloned.1.call-start = ((), (), s32[]{:S(2)}) async-start(), calls=%async_computation.8 | async-start | bytes 3244032 | tf_op jit(solution)/shard_map/all_gather | solution.py:10
  7.3 120.5 %all-gather.9.cloned.1.call-start = ((), (), s32[]{:S(2)}) async-start(), calls=%async_computation.2 | async-start | bytes 3244032 | tf_op jit(solution)/shard_map/all_gather | solution.py:18
  8.0 177.9 %all-gather.11.cloned.1.call-start = ((), (), s32[]{:S(2)}) async-start(), calls=%async_computation.3 | async-start | bytes 3244032 | tf_op jit(solution)/shard_map/all_gather | solution.py:18
  8.7 235.1 %all-gather.19.cloned.1.call-start = ((), (), s32[]{:S(2)}) async-start(), calls=%async_computation.9 | async-start | bytes 3244032 | tf_op jit(solution)/shard_map/all_gather | solution.py:10
  9.3 243.2 %reduce-scatter.3.cloned.1.call-start = ((), (), s32[]{:S(2)}) async-start(), calls=%async_computation.4 | async-start | bytes 786432 | tf_op jit(solution)/shard_map/reduce_scatter | solution.py:76
  190.7 122.3 %all-gather.13.cloned.1.call-start = ((), (), s32[]{:S(2)}) async-start(), calls=%async_computation.5 | async-start | bytes 3244032 | tf_op jit(solution)/shard_map/all_gather | solution.py:18
  191.3 179.8 %all-gather.15.cloned.1.call-start = ((), (), s32[]{:S(2)}) async-start(), calls=%async_computation.6 | async-start | bytes 3244032 | tf_op jit(solution)/shard_map/all_gather | solution.py:18
  192.1 190.8 %reduce-scatter.5.cloned.1.call-start = ((), (), s32[]{:S(2)}) async-start(), calls=%async_computation.7 | async-start | bytes 786432 | tf_op jit(solution)/shard_map/reduce_scatter | solution.py:87
  243.8 8.7 %copy-start = (bf16[128,1024]{1,0:T(8,128)(2,1)S(1)}, bf16[128,1024]{1,0:T(8,128)(2,1)}, u32[]{:S(2)}) copy-start(bf16[128,1024]{1,0:T(8,128)(2,1)} %param.11) | copy-start | bytes 786436
  243.9 69.2 %copy-start.1 = (f32[1024]{0:T(1024)S(1)}, f32[1024]{0:T(1024)}, u32[]{:S(2)}) copy-start(f32[1024]{0:T(1024)} %param.17) | copy-start | bytes 12292
  371.2 15.3 %copy-start.2 = (f32[512]{0:T(512)S(1)}, f32[512]{0:T(512)}, u32[]{:S(2)}) copy-start(f32[512]{0:T(512)} %param.21) | copy-start | bytes 6148
Sparse Core Ops, SparseCore 0:
  9.5 60.0 all-gather.16
  71.8 55.9 all-gather.8
  129.9 55.9 all-gather.10
  187.9 55.9 all-gather.18
  245.9 6.5 reduce-scatter.2
  254.6 58.4 all-gather.12
  315.2 55.9 all-gather.14
  376.2 6.5 reduce-scatter.4
